TPU v7x, 256 devices: a 8x8x2 block of a 8x8x16 slice. The times are simulated.
256 devices in a mesh: grp: 2 (over z), sp: 16 (over y, core), tp: 8 (over x).
Axes of the slice: x: 8, y: 8, z: 2, core: 2. Of those that a mesh axis runs over, the one named last changes fastest.
The devices are a block of a 8x8x16 slice.
Arguments:
- resid_in: bfloat16 [32768, 2048], P(('grp', 'sp', 'tp')), parts along dimension 0, may hold values from -6 to 6
- pool_input: bfloat16 [32768, 1024], P(('grp', 'sp'), 'tp'), parts along dimension 0, may hold values from -6 to 6
- pool_weight: bfloat16 [4, 256, 256], replicated, may hold values from -0.375 to 0.375
- pool_scale: float32 [1024], replicated, may hold values from 0.2 to 0.8
- out_weight: bfloat16 [1024, 2048], replicated, may hold values from -0.1875 to 0.1875
- mix_gain: float32 [2048], replicated, may hold values from 0.1 to 1.9
- ffn_gain: float32 [2048], replicated, may hold values from 0.1 to 1.9
- w_gate: bfloat16 [32, 2048, 1024], P('sp', None, 'tp'), may hold values from -0.375 to 0.375
- w_up: bfloat16 [32, 2048, 1024], P('sp', None, 'tp'), may hold values from -0.375 to 0.375
- w_down: bfloat16 [32, 1024, 2048], P('sp', 'tp'), may hold values from -0.1875 to 0.1875
- routes: int32 [32768, 2], P(('grp', 'sp', 'tp')), parts along dimension 0, may hold values from 0 to 31, all different within a row; in each aligned block of 128 rows (0 to 127, 128 to 255, ...) at most 9 rows name the same one
- route_weight: float32 [32768, 2], P(('grp', 'sp', 'tp')), parts along dimension 0, may hold values from 0.1 to 1
- post_gain: float32 [2048], replicated, may hold values from 0.1 to 1.9
Outputs:
- layer_out: bfloat16 [32768, 2048], P(('grp', 'sp', 'tp')), parts along dimension 0
There are 2 independent parts, one for each index of `grp`. A program takes and returns all parts, laid end to end along the dimension named above; an argument that names none is the same for every part. Nothing has to cross between parts.
Inputs may be any that keep to these rules, and one draw needn't show every extreme that they name: `routes`: each row names 2 different experts. The rows of one device name any one expert at most 9 times, and in every draw some device's rows name some expert exactly 9 times.
All inputs are finite; a program needn't handle non-finite values.
Results may differ from a plain program's by a relative error of at most 0.011.
Values may be sent and summed in bfloat16 or wider, within the bound.
A program may use at most 128 MiB of HBM per device.

v0:
```python
import jax
import jax.numpy as jnp
from jax import lax
from jax.sharding import PartitionSpec as P

GROUPS = 4
GROUP_DIM = 256
TOP = 2
CAP = 9


pool_windows = (2, 4, 8, 16)
reach_back = 15
norm_eps = 1e-06
clamp_limit = 7.0
glu_alpha = 1.702


def passed_along(x, axis, by):
    size = lax.axis_size(axis)
    pairs = [(i, i + by) for i in range(size) if 0 <= i + by < size]
    return lax.ppermute(x, axis, pairs)


def rms_scale(values, gain_vec):
    inverse = lax.rsqrt(jnp.mean(values * values, axis=-1, keepdims=True) + norm_eps)
    return values * inverse * gain_vec


def clamped_unit(gate_pre, upward):
    gate_clip = jnp.minimum(gate_pre, clamp_limit)
    linear = jnp.clip(upward, -clamp_limit, clamp_limit)
    return gate_clip * jax.nn.sigmoid(glu_alpha * gate_clip) * (linear + 1.0)


def per_device(
    resid_in,
    pool_input,
    pool_weight,
    pool_scale,
    out_weight,
    mix_gain,
    ffn_gain,
    w_gate,
    w_up,
    w_down,
    routes,
    route_weight,
    post_gain,
):
    n_sp = lax.axis_size("sp")
    n_tp = lax.axis_size("tp")
    seg_rows, channels = pool_input.shape
    last_rows = pool_input[seg_rows - reach_back :]
    before = passed_along(last_rows, "sp", 1)
    extended = jnp.concatenate([before, pool_input], axis=0).astype(jnp.float32)
    first_chan = lax.axis_index("tp") * channels
    chan_group = (first_chan + lax.iota(jnp.int32, channels)) // GROUP_DIM
    positions = lax.axis_index("sp") * seg_rows + lax.iota(jnp.int32, seg_rows)
    window = jnp.zeros((channels,), jnp.int32)
    for group_level, win_len in enumerate(pool_windows):
        window = jnp.where(chan_group == group_level, win_len, window)
    running = jnp.zeros((seg_rows, channels), jnp.float32)
    window_sum = running
    for offset in range(pool_windows[-1]):
        running = running + extended[reach_back - offset : reach_back - offset + seg_rows]
        if offset + 1 in pool_windows:
            window_sum = jnp.where(window[None, :] == offset + 1, running, window_sum)
    divisor = jnp.minimum(positions[:, None] + 1, window[None, :]).astype(jnp.float32)
    mixed_rows = (window_sum / divisor - extended[reach_back:]).astype(jnp.bfloat16)
    token_mixed = lax.all_to_all(mixed_rows, "tp", split_axis=0, concat_axis=1, tiled=True)
    tok_rows = token_mixed.shape[0]
    pooled = jnp.einsum(
        "tgc,gcd->tgd",
        token_mixed.reshape(tok_rows, GROUPS, GROUP_DIM),
        pool_weight,
        preferred_element_type=jnp.float32,
    )
    pooled = (
        (pooled * pool_scale.reshape(GROUPS, GROUP_DIM)).astype(jnp.bfloat16).reshape(tok_rows, -1)
    )
    mix_out = jnp.dot(pooled, out_weight, preferred_element_type=jnp.float32)
    residual = (resid_in.astype(jnp.float32) + rms_scale(mix_out, mix_gain)).astype(jnp.bfloat16)
    normed = rms_scale(residual.astype(jnp.float32), ffn_gain).astype(jnp.bfloat16)
    width = normed.shape[1]
    local_experts = w_gate.shape[0]
    n_experts = local_experts * n_sp
    slot_total = n_experts * CAP
    flat_route = routes.reshape(-1)
    onehot = (flat_route[:, None] == lax.iota(jnp.int32, n_experts)[None, :]).astype(jnp.int32)
    slot_rank = jnp.sum((jnp.cumsum(onehot, axis=0) - onehot) * onehot, axis=1)
    slot_index = flat_route * CAP + slot_rank
    picker = slot_index[:, None] == lax.iota(jnp.int32, slot_total)[None, :]
    picker_rows = picker.astype(jnp.bfloat16)
    token_pick = jnp.sum(
        picker.reshape(tok_rows, TOP, slot_total).astype(jnp.float32), axis=1
    ).astype(jnp.bfloat16)
    buffer = lax.dot_general(
        token_pick, normed, (((0,), (0,)), ((), ())), preferred_element_type=jnp.float32
    )
    outgoing = buffer.astype(jnp.bfloat16).reshape(n_sp, local_experts * CAP, width)
    at_owner = lax.all_to_all(outgoing, "sp", split_axis=0, concat_axis=0, tiled=True)
    arrived = lax.all_gather(at_owner[:, None], "tp", axis=1, tiled=True)
    arrived = arrived.reshape(n_sp, n_tp, local_experts, CAP, width)
    gate_pre = jnp.einsum("sklcd,ldf->sklcf", arrived, w_gate, preferred_element_type=jnp.float32)
    upward = jnp.einsum("sklcd,ldf->sklcf", arrived, w_up, preferred_element_type=jnp.float32)
    activated = clamped_unit(gate_pre, upward).astype(jnp.bfloat16)
    terms = jnp.einsum("sklcf,lfd->kslcd", activated, w_down, preferred_element_type=jnp.float32)
    summed = lax.psum_scatter(
        terms.reshape(1 * lax.axis_size("tp"), n_sp, local_experts * CAP, width).astype(
            jnp.bfloat16
        ),
        "tp",
        scatter_dimension=0,
        tiled=True,
    ).astype(jnp.float32)
    results = summed[0].astype(jnp.bfloat16)
    returned = lax.all_to_all(results, "sp", split_axis=0, concat_axis=0, tiled=True).reshape(
        slot_total, width
    )
    gathered = jnp.dot(picker_rows, returned, preferred_element_type=jnp.float32)
    expert_mix = jnp.sum(gathered.reshape(tok_rows, TOP, width) * route_weight[:, :, None], axis=1)
    return (residual.astype(jnp.float32) + rms_scale(expert_mix, post_gain)).astype(jnp.bfloat16)


def solution(mesh):
    in_specs = (
        P(("grp", "sp", "tp"), None),
        P(("grp", "sp"), "tp"),
        P(),
        P(),
        P(),
        P(),
        P(),
        P("sp", None, "tp"),
        P("sp", None, "tp"),
        P("sp", "tp", None),
        P(("grp", "sp", "tp"), None),
        P(("grp", "sp", "tp"), None),
        P(),
    )
    out_specs = P(("grp", "sp", "tp"), None)
    return jax.shard_map(
        per_device, mesh=mesh, in_specs=in_specs, out_specs=out_specs, check_vma=False
    )
```

profile of v0, /device:TPU:513, one launch (start us, length us, event | category | flops | bytes accessed | tf_op | source)
XLA Modules:
  0.0 397.1 jit_solution(8766756153125260866)
XLA Ops:
  7.3 5.7 %collective-permute-start = (bf16[15,128]{1,0:T(8,128)(2,1)S(1)}, bf16[15,128]{1,0:T(8,128)(2,1)S(1)}, u32[]{:S(2)}, u32[]{:S(2)}) collective-permute-start(bf16[15,128]{1,0:T(8,128)(2,1)S(1)} %slice.58), channel_id=1, source_target_pairs={{0,8},{8,16},{16,24},{24,32},{32,40},{40,48},{48,56},{56,64},{64,7... | collective-permute-start | bytes 11528 | tf_op jit(solution)/shard_map/ppermute | solution.py:22
  13.1 0.8 copy.76
  14.7 15.0 %collective-permute-done = bf16[15,128]{1,0:T(8,128)(2,1)S(1)} collective-permute-done((bf16[15,128]{1,0:T(8,128)(2,1)S(1)}, bf16[15,128]{1,0:T(8,128)(2,1)S(1)}, u32[]{:S(2)}, u32[]{:S(2)}) %collective-permute-start) | collective-permute-done | bytes 3872 | tf_op jit(solution)/shard_map/ppermute | solution.py:22
  29.7 1.0 maximum_convert_fusion
  30.7 1.5 fusion.42
  32.2 3.7 all-to-all-start
  36.8 9.4 %all-to-all-done = bf16[8,128,128]{2,1,0:T(8,128)(2,1)S(1)} async-done(((bf16[8,128,128]{2,1,0:T(8,128)(2,1)}), bf16[8,128,128]{2,1,0:T(8,128)(2,1)S(1)}, u32[]{:S(2)}, u32[]{:S(2)}) %all-to-all-start) | async-done | bytes 262176 | tf_op jit(solution)/shard_map/all_to_all | solution.py:71
  46.9 3.1 multiply_reduce_fusion.1
  50.7 1.6 convolution_convert_fusion
  52.2 1.4 reshape.162
  53.7 44.4 %all_to_all.26 = bf16[16,18,2048]{2,1,0:T(8,128)(2,1)S(1)} all-to-all(bf16[16,18,2048]{2,1,0:T(8,128)(2,1)S(1)} %reshape.162), channel_id=1, replica_groups=mesh['grp'=2,'sp'=16,'tp'=8] {'sp'}, dimensions={0} | all-to-all | bytes 2359296 | tf_op jit(solution)/shard_map/all_to_all | solution.py:102
  98.1 1.7 copy.80
  100.1 104.1 %all-gather.3.cloned.1.call-done = bf16[16,144,2048]{2,0,1:T(8,128)(2,1)} async-done(((bf16[16,18,2048]{2,0,1:T(8,128)(2,1)}), bf16[16,144,2048]{2,0,1:T(8,128)(2,1)}) %all-gather.3.cloned.1.call-update) | async-done | bytes 9437200 | tf_op jit(solution)/shard_map/all_gather | solution.py:103
  204.2 5.3 %fusion.20 = f32[16,8,2,9,128]{4,0,3,1,2:T(8,128)S(1)} fusion(bf16[16,8,2,9,2048]{4,0,3,2,1:T(8,128)(2,1)} %bitcast.67, bf16[2,2048,128]{2,1,0:T(8,128)(2,1)S(1)} %copy-done.9), kind=kOutput, calls=%fused_computation.16 | convolution fusion | flops 1208254464 | bytes 11665408 | tf_op jit(solution)/shard_map/sklcd,ldf->sklcf/dot_general | solution.py:105
  209.5 1.1 copy-done.8
  210.9 2.8 fusion.23
  213.7 5.1 %convert_bitcast_fusion = bf16[8,16,2,9,2048]{4,0,3,1,2:T(8,128)(2,1)} fusion(bf16[2,128,2048]{2,1,0:T(8,128)(2,1)S(1)} %copy-done, bf16[16,8,2,9,128]{4,0,3,1,2:T(8,128)(2,1)S(1)} %fusion.23), kind=kOutput, calls=%fused_computation | convolution fusion | flops 1212678144 | bytes 11075584 | tf_op jit(solution)/shard_map/sklcf,lfd->kslcd/dot_general | solution.py:108
  218.8 12.5 %copy.84 = bf16[8,16,2,9,2048]{4,1,3,2,0:T(8,128)(2,1)} copy(bf16[8,16,2,9,2048]{4,0,3,1,2:T(8,128)(2,1)} %convert_bitcast_fusion) | data formatting | bytes 18874368 | tf_op jit(solution)/shard_map/convert_element_type | solution.py:110
  231.3 105.1 %reduce-scatter.2.cloned.1.call-done = bf16[1,16,18,2048]{3,1,2,0:T(8,128)(2,1)} async-done(((bf16[8,16,18,2048]{3,1,2,0:T(8,128)(2,1)}), bf16[1,16,18,2048]{3,1,2,0:T(8,128)(2,1)}) %reduce-scatter.2.cloned.1.call-update) | async-done | bytes 1179664 | tf_op jit(solution)/shard_map/reduce_scatter | solution.py:109
  336.5 2.0 copy.85
  338.5 47.2 %all_to_all.27 = bf16[16,18,2048]{2,1,0:T(8,128)(2,1)S(1)} all-to-all(bf16[16,18,2048]{2,1,0:T(8,128)(2,1)S(1)} %copy.85), channel_id=1, replica_groups=mesh['grp'=2,'sp'=16,'tp'=8] {'sp'}, dimensions={0} | all-to-all | bytes 2359296 | tf_op jit(solution)/shard_map/all_to_all | solution.py:118
  385.7 1.2 reshape.170
  386.9 2.1 fusion.4
  389.2 1.0 fusion.31
  (53 shorter events, 4.5 us)
Async XLA Ops:
  6.5 207.2 %copy-start = (bf16[2,128,2048]{2,1,0:T(8,128)(2,1)S(1)}, bf16[2,128,2048]{2,1,0:T(8,128)(2,1)}, u32[]{:S(2)}) copy-start(bf16[2,128,2048]{2,1,0:T(8,128)(2,1)} %param.22) | copy-start | bytes 3145732
  7.3 22.4 %collective-permute-start = (bf16[15,128]{1,0:T(8,128)(2,1)S(1)}, bf16[15,128]{1,0:T(8,128)(2,1)S(1)}, u32[]{:S(2)}, u32[]{:S(2)}) collective-permute-start(bf16[15,128]{1,0:T(8,128)(2,1)S(1)} %slice.58), channel_id=1, source_target_pairs={{0,8},{8,16},{16,24},{24,32},{32,40},{40,48},{48,56},{56,64},{64,7... | collective-permute-start | bytes 11528 | tf_op jit(solution)/shard_map/ppermute | solution.py:22
  30.7 5.7 %copy-start.7 = (f32[1024]{0:T(1024)S(1)}, f32[1024]{0:T(1024)}, u32[]{:S(2)}) copy-start(f32[1024]{0:T(1024)} %param.16) | copy-start | bytes 12292
  30.7 6.0 %copy-start.6 = (s32[128,2]{0,1:T(2,128)S(1)}, s32[128,2]{0,1:T(2,128)}, u32[]{:S(2)}) copy-start(s32[128,2]{0,1:T(2,128)} %param.23) | copy-start | bytes 3076
  32.2 14.2 %copy-start.1 = (bf16[4,256,256]{2,1,0:T(8,128)(2,1)S(1)}, bf16[4,256,256]{2,1,0:T(8,128)(2,1)}, u32[]{:S(2)}) copy-start(bf16[4,256,256]{2,1,0:T(8,128)(2,1)} %param.15) | copy-start | bytes 1572868
  32.2 14.0 %all-to-all-start = ((bf16[8,128,128]{2,1,0:T(8,128)(2,1)}), bf16[8,128,128]{2,1,0:T(8,128)(2,1)S(1)}, u32[]{:S(2)}, u32[]{:S(2)}) async-start(bf16[8,128,128]{2,1,0:T(8,128)(2,1)} %bitcast), calls=%async_computation | async-start | bytes 524288 | tf_op jit(solution)/shard_map/all_to_all | solution.py:71
  36.0 168.2 %all-gather.3.cloned.1.call-start = ((), (), s32[]{:S(2)}) async-start(), calls=%async_computation.5 | async-start | bytes 10616832 | tf_op jit(solution)/shard_map/all_gather | solution.py:103
  46.9 3.1 copy-start.2
  46.9 3.1 copy-start.3
  50.0 0.7 copy-start.4
  99.8 104.4 %copy-start.9 = (bf16[2,2048,128]{2,1,0:T(8,128)(2,1)S(1)}, bf16[2,2048,128]{2,1,0:T(8,128)(2,1)}, u32[]{:S(2)}) copy-start(bf16[2,2048,128]{2,1,0:T(8,128)(2,1)} %param.20) | copy-start | bytes 3145732
  99.8 236.6 %reduce-scatter.2.cloned.1.call-start = ((), (), s32[]{:S(2)}) async-start(), calls=%async_computation.4 | async-start | bytes 10616832 | tf_op jit(solution)/shard_map/reduce_scatter | solution.py:109
  204.2 6.4 %copy-start.8 = (bf16[16,144,2048]{2,0,1:T(8,128)(2,1)S(1)}, bf16[16,144,2048]{2,0,1:T(8,128)(2,1)}, u32[]{:S(2)}) copy-start(bf16[16,144,2048]{2,0,1:T(8,128)(2,1)} %all-gather.3.cloned.1.call-done) | copy-start | bytes 28311556
  204.2 6.7 %copy-start.10 = (bf16[2,2048,128]{2,1,0:T(8,128)(2,1)S(1)}, bf16[2,2048,128]{2,1,0:T(8,128)(2,1)}, u32[]{:S(2)}) copy-start(bf16[2,2048,128]{2,1,0:T(8,128)(2,1)} %param.21) | copy-start | bytes 3145732
  385.7 1.2 copy-start.11
  386.9 2.3 copy-start.5
Sparse Core Ops, SparseCore 0:
  100.0 104.1 all-gather.2
  231.5 104.9 reduce-scatter.1
where the time goes:
time: 398 us; the launch traced here: 397 us
  waiting for transfers between devices  234 us (59%)
  blocking collectives  91.7 us (23%)
  local copies, waits for them, and re-layouts  23 us (6%)
  matrix products  20.2 us (5%)
  between operations  13.7 us (3%)
  starting transfers between devices  9.79 us (2%)
  other arithmetic  4.91 us (1%)
    reduce_scatter x1, waiting for transfers between devices, per_device(): lax.psum_scatter(terms.reshape(1 * lax.axis_size('tp'), n_sp, local_exper...  105 us
    all_gather x1, waiting for transfers between devices, per_device(): arrived = lax.all_gather(at_owner[:, None], 'tp', axis=1, tiled=True)  104 us
    all_to_all x1, blocking collectives, per_device(): lax.all_to_all(results, 'sp', split_axis=0, concat_axis=0, tiled=True)  47.2 us
    all_to_all x1, blocking collectives, per_device(): lax.all_to_all(outgoing, 'sp', split_axis=0, concat_axis=0, tiled=True)  44.4 us
    ppermute x1, waiting for transfers between devices, passed_along(): return lax.ppermute(x, axis, pairs)  15 us
    convert_element_type x1, local copies, waits for them, and re-layouts, per_device(): terms.reshape(1 * lax.axis_size('tp'), n_sp, local_experts * CAP, width)  12.5 us
    all_to_all x1, waiting for transfers between devices, per_device(): lax.all_to_all(mixed_rows, 'tp', split_axis=0, concat_axis=1, tiled=True)  9.42 us
  transfers between devices with their start and end apart: 4, of which 4 were waited for; matrix products, arithmetic and copies ran while one was open for 1% of the time, Pallas kernels for 0%

commit v1 on v0

v1 whole, which is shorter than its diff:
```python
import functools

import jax
import jax.numpy as jnp
from jax import lax
from jax.experimental import pallas as pl
from jax.experimental.pallas import tpu as pltpu
from jax.sharding import PartitionSpec as P

GROUPS = 4
GROUP_DIM = 256
TOP = 2
CAP = 9
MAIN = 8
CORES = 2

pool_windows = (2, 4, 8, 16)
halo_rows = 16
norm_eps = 1e-06
clamp_limit = 7.0
glu_alpha = 1.702
MESH = pl.DeviceIdType.MESH
F32 = jnp.float32
BF16 = jnp.bfloat16


def dot(a, b):
    return jnp.dot(a, b, preferred_element_type=F32)


def rows_of(block):
    wide = block.astype(F32)
    return wide.reshape(-1, wide.shape[-1]).astype(BF16)


def kernel(
    n_sp, n_tp,
    pin, resid, pool_w, pool_s, out_w, mix_g, ffn_g, w_gate, w_up, w_down, routes, route_w, post_g,
    out,
    ext, mixbuf, tokmix, pool_wv, out_wv, pooled, wide, resbuf, normbuf, whi, wlo,
    disp, yarr, ovout, wgu, wd, rows, xb, act, orow, ret, ovback, fin, outbuf,
    lsem, halo_s, halo_r, pool_sem_s, pool_sem_r, w_s, w_r, f_s, f_r,
    y_s, y_r, x_s, x_r, o_s, o_r, b_s, b_r, v_s, v_r,
):
    n_y = n_sp // CORES
    local_experts = w_gate.shape[0]
    row_experts = local_experts * CORES
    blocks = row_experts + 1
    slots_row = blocks * 8
    step = n_tp // row_experts
    seg, channels = pin.shape
    tok, width = resid.shape
    ff = w_gate.shape[2]
    sp = lax.axis_index("sp")
    tp = lax.axis_index("tp")
    y = sp // CORES
    core = sp % CORES
    par = y % step
    mine = tp // step
    active = tp % step == par
    mate = y * CORES + (1 - core)

    def home(j):
        return j * step + par

    def at_y(row):
        return row * CORES + core

    def remote(src, dst, send, recv, **where):
        return pltpu.make_async_remote_copy(
            src_ref=src, dst_ref=dst, send_sem=send, recv_sem=recv, device_id=where, device_id_type=MESH
        )

    def landed(dst, sem):
        pltpu.make_async_copy(dst, dst, sem).wait()

    loads = [
        pltpu.make_async_copy(pin, ext.at[pl.ds(halo_rows, seg)], lsem.at[0]),
        pltpu.make_async_copy(pool_w, pool_wv, lsem.at[1]),
        pltpu.make_async_copy(out_w, out_wv, lsem.at[2]),
        pltpu.make_async_copy(resid, resbuf, lsem.at[3]),
    ]
    for load in loads:
        load.start()

    barrier = pltpu.get_barrier_semaphore()
    for d in range(1, n_tp):
        pl.semaphore_signal(barrier, inc=1, device_id={"tp": (tp + d) % n_tp}, device_id_type=MESH)
    for d in range(1, n_y):
        pl.semaphore_signal(barrier, inc=1, device_id={"sp": at_y((y + d) % n_y)}, device_id_type=MESH)
    beside = (sp + 2 * core - 1 + n_sp) % n_sp
    pl.semaphore_signal(barrier, inc=1, device_id={"sp": mate}, device_id_type=MESH)
    pl.semaphore_signal(barrier, inc=1, device_id={"sp": beside}, device_id_type=MESH)
    pl.semaphore_wait(barrier, n_tp + n_y)

    halo = remote(
        pin.at[pl.ds(seg - halo_rows, halo_rows)], ext.at[pl.ds(0, halo_rows)], halo_s, halo_r, sp=(sp + 1) % n_sp
    )
    halo.start()
    loads[0].wait()
    halo.wait()
    at = lax.broadcasted_iota(jnp.int32, (halo_rows + seg, 1), 0)
    own = ext[...].astype(F32)
    own = jnp.where(jnp.logical_and(at < halo_rows, sp == 0), 0.0, own)
    group = tp * channels // GROUP_DIM
    total, picked = own, own
    for level, window in enumerate(pool_windows):
        total = total + pltpu.roll(total, window // 2, 0)
        picked = jnp.where(group == level, total, picked)
    window = lax.shift_left(jnp.int32(2), group.astype(jnp.int32))
    divisor = jnp.minimum(sp * seg + at - halo_rows + 1, window).astype(F32)
    mixed = picked / jnp.maximum(divisor, 1.0) - own
    mixbuf[...] = mixed[halo_rows:].astype(BF16)

    def pool_copy(d):
        to = (tp + d) % n_tp
        return remote(
            mixbuf.at[pl.ds(to * tok, tok)], tokmix.at[tp], pool_sem_s.at[d], pool_sem_r.at[d], tp=to
        )

    keep = pltpu.make_async_copy(mixbuf.at[pl.ds(tp * tok, tok)], tokmix.at[tp], pool_sem_r.at[0])
    keep.start()
    for d in range(1, n_tp):
        pool_copy(d).start()

    def weight_copies(e):
        col = home(core * local_experts + e)
        half = [pl.ds(0, ff), pl.ds(ff, ff)]
        pairs = [
            (w_gate.at[e], wgu.at[tp, :, half[0]]),
            (w_up.at[e], wgu.at[tp, :, half[1]]),
            (w_down.at[e], wd.at[pl.ds(tp * ff, ff)]),
        ]
        far = lambda: [remote(s, t, w_s.at[e, i], w_r.at[i, tp], tp=col) for i, (s, t) in enumerate(pairs)]
        near = lambda: [pltpu.make_async_copy(s, t, w_r.at[i, tp]) for i, (s, t) in enumerate(pairs)]
        return col, far, near

    for e in range(local_experts):
        col, far, near = weight_copies(e)

        @pl.when(col != tp)
        def _():
            for copy in far():
                copy.start()

        @pl.when(col == tp)
        def _():
            for copy in near():
                copy.start()

    lanes = whi.shape[1]
    expert_lane = lax.broadcasted_iota(jnp.int32, (tok, 128), 1)
    before = (
        lax.broadcasted_iota(jnp.int32, (tok, tok), 1) < lax.broadcasted_iota(jnp.int32, (tok, tok), 0)
    ).astype(F32).astype(BF16)
    named = [routes[:, k : k + 1] for k in range(TOP)]
    onehot = [(named[k] == expert_lane).astype(F32) for k in range(TOP)]
    earlier = jnp.zeros((1, 128), F32)
    slot_lane = lax.broadcasted_iota(jnp.int32, (1, lanes), 1)
    inside = slot_lane % slots_row
    spill = inside >= row_experts * MAIN
    row_expert = jnp.where(spill, inside - row_experts * MAIN, inside // MAIN)
    slot_rank = jnp.where(spill, MAIN, inside % MAIN).astype(F32)
    valid = jnp.logical_and(row_expert < row_experts, slot_lane < n_y * slots_row)
    slot_expert = jnp.where(valid, slot_lane // slots_row * row_experts + row_expert, -1)
    pick = jnp.zeros((tok, lanes), F32)
    comb = jnp.zeros((tok, lanes), F32)
    for k in range(TOP):
        ranks = dot(before, onehot[k].astype(BF16)) + earlier
        rank = jnp.sum(ranks * onehot[k], axis=1, keepdims=True)
        earlier = earlier + jnp.sum(onehot[k], axis=0, keepdims=True)
        hit = jnp.logical_and(named[k] == slot_expert, rank == slot_rank).astype(F32)
        pick = pick + hit
        comb = comb + hit * route_w[:, k : k + 1]
    high = comb.astype(BF16)
    whi[...] = high
    wlo[...] = (comb - high.astype(F32)).astype(BF16)
    pick_rows = jnp.transpose(pick)[: n_y * slots_row].astype(BF16)

    keep.wait()
    for d in range(1, n_tp):
        pool_copy(d).wait()
    loads[1].wait()
    per = GROUP_DIM // channels
    for g in range(GROUPS):
        mixed_g = jnp.concatenate([tokmix[g * per + i] for i in range(per)], axis=1)
        cols = slice(g * GROUP_DIM, (g + 1) * GROUP_DIM)
        pooled[:, cols] = (dot(mixed_g, pool_wv[g]) * pool_s[:, cols]).astype(BF16)
    loads[2].wait()
    tile = 256

    @pl.loop(0, width // tile)
    def _(n):
        cols = pl.ds(pl.multiple_of(n * tile, tile), tile)
        wide[:, cols] = dot(pooled[...], out_wv[:, cols])

    loads[3].wait()
    part = 32

    def scaled(values, gain):
        inverse = lax.rsqrt(jnp.mean(values * values, axis=-1, keepdims=True) + norm_eps)
        return values * inverse * gain[...]

    @pl.loop(0, tok // part)
    def _(r):
        at = pl.ds(pl.multiple_of(r * part, part), part)
        residual = (resbuf[at, :].astype(F32) + scaled(wide[at, :], mix_g)).astype(BF16)
        resbuf[at, :] = residual
        normbuf[at, :] = scaled(residual.astype(F32), ffn_g).astype(BF16)

    @pl.loop(0, width // tile)
    def _(n):
        cols = pl.ds(pl.multiple_of(n * tile, tile), tile)
        sent = dot(pick_rows, normbuf[:, cols])
        disp[:, :, :, cols] = sent.reshape(n_y, blocks, 8, tile).astype(BF16)

    def y_copy(d):
        to = (y + d) % n_y
        return remote(disp.at[to], yarr.at[y], y_s.at[d], y_r.at[d], sp=at_y(to))

    y_keep = pltpu.make_async_copy(disp.at[y], yarr.at[y], y_r.at[0])
    y_keep.start()
    for d in range(1, n_y):
        y_copy(d).start()
    y_keep.wait()
    for d in range(1, n_y):
        y_copy(d).wait()

    count = n_y * 8
    to_row = lax.broadcasted_iota(jnp.int32, (row_experts * n_y, count), 0)
    from_row = lax.broadcasted_iota(jnp.int32, (row_experts * n_y, count), 1)
    regroup = (from_row == to_row % n_y * 8 + to_row // n_y).astype(F32).astype(BF16)

    @pl.loop(0, width // tile)
    def _(n):
        cols = pl.ds(pl.multiple_of(n * tile, tile), tile)
        moved = dot(regroup, rows_of(yarr[:, row_experts, :, cols]))
        ovout[:, :, cols] = moved.reshape(row_experts, n_y, tile).astype(BF16)

    def x_copies(k):
        j = (mine + 1 + k) % row_experts
        col = home(j)
        pairs = [(yarr.at[:, j], rows.at[tp, pl.ds(0, n_y)]), (ovout.at[j], rows.at[tp, n_y])]
        far = lambda: [remote(s, t, x_s.at[k, i], x_r.at[i, tp], tp=col) for i, (s, t) in enumerate(pairs)]
        near = lambda: [pltpu.make_async_copy(s, t, x_r.at[i, tp]) for i, (s, t) in enumerate(pairs)]
        return col, far, near

    for k in range(row_experts):
        col, far, near = x_copies(k)

        @pl.when(col != tp)
        def _():
            for copy in far():
                copy.start()

        @pl.when(col == tp)
        def _():
            for copy in near():
                copy.start()

    owner = mine // local_experts == core

    def forward_copies(s):
        shard = pl.ds(s * ff, ff)
        return [
            remote(wgu.at[s], wgu.at[s], f_s.at[0, s], f_r.at[0, s], sp=mate),
            remote(wd.at[shard], wd.at[shard], f_s.at[1, s], f_r.at[1, s], sp=mate),
        ]

    @pl.when(jnp.logical_and(active, owner))
    def _():
        for d in (0, 1, -1, 2, -2, 3, -3, 4):
            s = (tp + d + n_tp) % n_tp
            landed(wgu.at[s, :, pl.ds(0, ff)], w_r.at[0, s])
            landed(wgu.at[s, :, pl.ds(ff, ff)], w_r.at[1, s])
            landed(wd.at[pl.ds(s * ff, ff)], w_r.at[2, s])
            for copy in forward_copies(s):
                copy.start()

    @pl.when(jnp.logical_and(active, jnp.logical_not(owner)))
    def _():
        for s in range(n_tp):
            landed(wgu.at[s], f_r.at[0, s])
            landed(wd.at[pl.ds(s * ff, ff)], f_r.at[1, s])

    def out_copy(s):
        return remote(orow.at[s], ret.at[mine], o_s.at[s], o_r.at[mine], tp=s)

    pair = 2
    held = n_y + 1

    @pl.when(active)
    def _():
        @pl.loop(0, n_tp // pair)
        def _(q):
            first = (tp + q * pair) % n_tp
            sources = [(first + i) % n_tp for i in range(pair)]
            for i, s in enumerate(sources):
                landed(rows.at[s, pl.ds(0, n_y)], x_r.at[0, s])
                landed(rows.at[s, n_y], x_r.at[1, s])
                xb[pl.ds(i * 8 * held, 8 * held), :] = rows_of(rows[s])

            @pl.loop(0, n_tp)
            def _(s):
                both = dot(xb[...], wgu[s])
                gate = jnp.minimum(both[:, :ff], clamp_limit)
                linear = jnp.clip(both[:, ff:], -clamp_limit, clamp_limit)
                cols = pl.ds(pl.multiple_of(s * ff, ff), ff)
                act[:, cols] = (gate * jax.nn.sigmoid(glu_alpha * gate) * (linear + 1.0)).astype(BF16)

            @pl.loop(0, width // tile)
            def _(n):
                cols = pl.ds(pl.multiple_of(n * tile, tile), tile)
                result = dot(act[...], wd[:, cols])
                for i, s in enumerate(sources):
                    piece = result[i * 8 * held : (i + 1) * 8 * held]
                    orow[s, :, :, cols] = piece.reshape(held, 8, tile).astype(BF16)

            for s in sources:
                @pl.when(s != tp)
                def _():
                    out_copy(s).start()

                @pl.when(s == tp)
                def _():
                    pltpu.make_async_copy(orow.at[s], ret.at[mine], o_r.at[mine]).start()

    for k in range(row_experts):
        landed(ret.at[k], o_r.at[k])
    to_row = lax.broadcasted_iota(jnp.int32, (count, row_experts * n_y), 0)
    from_row = lax.broadcasted_iota(jnp.int32, (count, row_experts * n_y), 1)
    regroup_back = (from_row == to_row % 8 * n_y + to_row // 8).astype(F32)
    regroup_back = jnp.where(to_row % 8 < row_experts, regroup_back, 0.0).astype(BF16)

    def b_copies(d):
        to = (y + d) % n_y
        main = lambda: remote(ret.at[:, to], fin.at[y, pl.ds(0, row_experts)], b_s.at[d], b_r.at[d], sp=at_y(to))
        over = lambda: remote(ovback.at[to], fin.at[y, row_experts], v_s.at[d], v_r.at[d], sp=at_y(to))
        return main, over

    b_keep = pltpu.make_async_copy(ret.at[:, y], fin.at[y, pl.ds(0, row_experts)], b_r.at[0])
    b_keep.start()
    for d in range(1, n_y):
        b_copies(d)[0]().start()

    @pl.loop(0, width // tile)
    def _(n):
        cols = pl.ds(pl.multiple_of(n * tile, tile), tile)
        moved = dot(regroup_back, rows_of(ret[:, n_y, :, cols]))
        ovback[:, :, cols] = moved.reshape(n_y, 8, tile).astype(BF16)

    v_keep = pltpu.make_async_copy(ovback.at[y], fin.at[y, row_experts], v_r.at[0])
    v_keep.start()
    for d in range(1, n_y):
        b_copies(d)[1]().start()
    b_keep.wait()
    v_keep.wait()
    for d in range(1, n_y):
        for copy in b_copies(d):
            copy().wait()

    @pl.loop(0, width // tile)
    def _(n):
        cols = pl.ds(pl.multiple_of(n * tile, tile), tile)
        came = rows_of(fin[:, :, :, cols])
        came = jnp.concatenate([came, jnp.zeros((lanes - n_y * slots_row, tile), BF16)], axis=0)
        wide[:, cols] = dot(whi[...], came) + dot(wlo[...], came)

    @pl.loop(0, tok // part)
    def _(r):
        at = pl.ds(pl.multiple_of(r * part, part), part)
        outbuf[at, :] = (resbuf[at, :].astype(F32) + scaled(wide[at, :], post_g)).astype(BF16)

    result = pltpu.make_async_copy(outbuf, out, lsem.at[0])
    result.start()

    for e in range(local_experts):
        col, far, near = weight_copies(e)

        @pl.when(col != tp)
        def _():
            for copy in far():
                copy.wait_send()

    for k in range(row_experts):
        col, far, near = x_copies(k)

        @pl.when(col != tp)
        def _():
            for copy in far():
                copy.wait_send()

    @pl.when(jnp.logical_and(active, owner))
    def _():
        for s in range(n_tp):
            for copy in forward_copies(s):
                copy.wait_send()

    @pl.when(active)
    def _():
        for s in range(n_tp):
            @pl.when(s != tp)
            def _():
                out_copy(s).wait_send()

    result.wait()


def per_device(
    resid_in, pool_input, pool_weight, pool_scale, out_weight, mix_gain, ffn_gain,
    w_gate, w_up, w_down, routes, route_weight, post_gain,
):
    n_sp = lax.axis_size("sp")
    n_tp = lax.axis_size("tp")
    n_y = n_sp // CORES
    seg, channels = pool_input.shape
    tok, width = resid_in.shape
    local_experts, _, ff = w_gate.shape
    row_experts = local_experts * CORES
    blocks = row_experts + 1
    slots = n_y * blocks * 8
    lanes = -(-slots // 128) * 128
    held = n_y + 1
    dma = pltpu.SemaphoreType.DMA
    vmem = pltpu.VMEM
    whole = pl.BlockSpec(memory_space=pltpu.VMEM)
    there = pl.BlockSpec(memory_space=pl.ANY)
    scratch = [
        vmem((halo_rows + seg, channels), BF16),
        vmem((seg, channels), BF16),
        vmem((n_tp, tok, channels), BF16),
        vmem(pool_weight.shape, BF16),
        vmem(out_weight.shape, BF16),
        vmem((tok, pool_scale.shape[0]), BF16),
        vmem((tok, width), F32),
        vmem((tok, width), BF16),
        vmem((tok, width), BF16),
        vmem((tok, lanes), BF16),
        vmem((tok, lanes), BF16),
        vmem((n_y, blocks, 8, width), BF16),
        vmem((n_y, blocks, 8, width), BF16),
        vmem((row_experts, 8, width), BF16),
        vmem((n_tp, width, 2 * ff), BF16),
        vmem((n_tp * ff, width), BF16),
        vmem((n_tp, held, 8, width), BF16),
        vmem((2 * held * 8, width), BF16),
        vmem((2 * held * 8, n_tp * ff), BF16),
        vmem((n_tp, held, 8, width), BF16),
        vmem((row_experts, held, 8, width), BF16),
        vmem((n_y, 8, width), BF16),
        vmem((n_y, blocks, 8, width), BF16),
        vmem((tok, width), BF16),
        dma((4,)), dma, dma, dma((n_tp,)), dma((n_tp,)),
        dma((local_experts, 3)), dma((3, n_tp)), dma((2, n_tp)), dma((2, n_tp)),
        dma((n_y,)), dma((n_y,)), dma((row_experts, 2)), dma((2, n_tp)),
        dma((n_tp,)), dma((row_experts,)), dma((n_y,)), dma((n_y,)), dma((n_y,)), dma((n_y,)),
    ]
    return pl.pallas_call(
        functools.partial(kernel, n_sp, n_tp),
        out_shape=jax.ShapeDtypeStruct((tok, width), BF16),
        in_specs=[there, there, there, whole, there, whole, whole, there, there, there, whole, whole, whole],
        out_specs=there,
        scratch_shapes=scratch,
        compiler_params=pltpu.CompilerParams(
            collective_id=0, has_side_effects=True, vmem_limit_bytes=60 * 1024 * 1024
        ),
    )(
        pool_input, resid_in, pool_weight, pool_scale[None], out_weight, mix_gain[None], ffn_gain[None],
        w_gate, w_up, w_down, routes, route_weight, post_gain[None],
    )


def solution(mesh):
    in_specs = (
        P(("grp", "sp", "tp"), None),
        P(("grp", "sp"), "tp"),
        P(),
        P(),
        P(),
        P(),
        P(),
        P("sp", None, "tp"),
        P("sp", None, "tp"),
        P("sp", "tp", None),
        P(("grp", "sp", "tp"), None),
        P(("grp", "sp", "tp"), None),
        P(),
    )
    out_specs = P(("grp", "sp", "tp"), None)
    return jax.shard_map(
        per_device, mesh=mesh, in_specs=in_specs, out_specs=out_specs, check_vma=False
    )
```

time: 398 us -> 252 us (0.63)
  Pallas kernels: 0 us -> 247 us
  waiting for transfers between devices: 234 us -> 0 us
  blocking collectives: 91.7 us -> 0 us
  matrix products: 20.2 us -> 0 us
  local copies, waits for them, and re-layouts: 23 us -> 4.7 us
  between operations: 13.7 us -> 0.01 us
  starting transfers between devices: 9.79 us -> 0 us
  other arithmetic: 4.91 us -> 0 us
    pallas_call x0 -> x1, Pallas kernels: none -> 247 us  [per_device(): pl.pallas_call(functools.partial(kernel, n_sp, n_tp), out_shape=jax.Shape...]
    reduce_scatter x1 -> x0, waiting for transfers between devices: 105 us -> none  [per_device(): lax.psum_scatter(terms.reshape(1 * lax.axis_size('tp'), n_sp, local_exper...]
    all_gather x1 -> x0, waiting for transfers between devices: 104 us -> none  [per_device(): arrived = lax.all_gather(at_owner[:, None], 'tp', axis=1, tiled=True)]
    all_to_all x2 -> x0, blocking collectives: 91.7 us -> none  [the longest x1 47.2 us: per_device(): lax.all_to_all(results, 'sp', split_axis=0, concat_axis=0, tiled=True)]
    dot_general x7 -> x0, matrix products: 20.2 us -> none  [the longest x1 5.33 us: per_device(): jnp.einsum('sklcd,ldf->sklcf', arrived, w_gate, preferred_element_type=jn...]
    ppermute x1 -> x0, waiting for transfers between devices: 15 us -> none  [passed_along(): return lax.ppermute(x, axis, pairs)]
    convert_element_type x3 -> x0, local copies, waits for them, and re-layouts: 14.7 us -> none  [the longest x1 12.5 us: per_device(): terms.reshape(1 * lax.axis_size('tp'), n_sp, local_experts * CAP, width)]
    all_to_all x1 -> x0, waiting for transfers between devices: 9.42 us -> none  [per_device(): lax.all_to_all(mixed_rows, 'tp', split_axis=0, concat_axis=1, tiled=True)]
  transfers between devices with their start and end apart: 4 -> 0, of which waited for: 4 -> 0; matrix products, arithmetic and copies ran while one was open for 1% -> 0% of each run, Pallas kernels for 0% -> 0%
where the time goes in v1:
time: 252 us; the launch traced here: 251 us
  Pallas kernels  247 us (98%)
  local copies, waits for them, and re-layouts  4.7 us (2%)
    pallas_call x1, Pallas kernels, per_device(): pl.pallas_call(functools.partial(kernel, n_sp, n_tp), out_shape=jax.Shape...  247 us

profile of v1, /device:TPU:513, one launch (start us, length us, event | category | flops | bytes accessed | tf_op | source)
XLA Modules:
  0.0 251.3 jit_solution(12921029648982408457)
XLA Ops:
  0.0 1.4 copy.14.routes
  1.4 1.4 copy.15.route_w
  2.8 246.6 %shard_map.127 = bf16[128,2048]{1,0:T(8,128)(2,1)} custom-call(bf16[1024,128]{1,0:T(8,128)(2,1)} %pin.1, bf16[128,2048]{1,0:T(8,128)(2,1)} %resid.1, bf16[4,256,256]{2,1,0:T(8,128)(2,1)} %pool_w.1, f32[1,1024]{1,0:T(1,128)} %bitcast.7, bf16[1024,2048]{1,0:T(8,128)(2,1)} %out_w.1, f32[1,2048]{1,0:T(1,128)} %bitcast.4, f32[1,2048]{1,0:T(1,128)} %bitcast.5, ...), custom_call_target="tpu_custom_call" | custom-call | tf_op jit(solution)/shard_map/pallas_call | solution.py:458
  249.4 1.9 copy.17

commit v2 on v0

v2 whole, which is shorter than its diff:
```python
import functools

import jax
import jax.numpy as jnp
from jax import lax
from jax.experimental import pallas as pl
from jax.experimental.pallas import tpu as pltpu
from jax.sharding import PartitionSpec as P

GROUPS = 4
GROUP_DIM = 256
TOP = 2
CAP = 9
MAIN = 8
CORES = 2

pool_windows = (2, 4, 8, 16)
halo_rows = 16
norm_eps = 1e-06
clamp_limit = 7.0
glu_alpha = 1.702
MESH = pl.DeviceIdType.MESH
F32 = jnp.float32
BF16 = jnp.bfloat16


def dot(a, b):
    return jnp.dot(a, b, preferred_element_type=F32)


def rows_of(block):
    wide = block.astype(F32)
    return wide.reshape(-1, wide.shape[-1]).astype(BF16)


def kernel(
    n_sp, n_tp,
    pin, resid, pool_w, pool_s, out_w, mix_g, ffn_g, w_gate, w_up, w_down, routes, route_w, post_g,
    out,
    ext, mixbuf, tokmix, pool_wv, out_wv, pooled, wide, resbuf, normbuf, whi, wlo,
    disp, yarr, ovout, wgu, wd, rows, xb, act, kept, given, taken, orow, ret, ovback, fin, outbuf,
    lsem, halo_s, halo_r, pool_sem_s, pool_sem_r, w_s, w_r, f_s, f_r,
    y_s, y_r, x_s, x_r, n_s, n_r, p_s, p_r, o_s, o_r, b_s, b_r, v_s, v_r,
):
    n_y = n_sp // CORES
    local_experts = w_gate.shape[0]
    row_experts = local_experts * CORES
    step = n_tp // row_experts
    near = n_tp // step
    blocks = row_experts + 1
    slots_row = blocks * 8
    held = n_y + 1
    seg, channels = pin.shape
    tok, width = resid.shape
    ff = w_gate.shape[2]
    tile = 256
    part = 32
    scope = jax.named_scope
    sp = lax.axis_index("sp")
    tp = lax.axis_index("tp")
    y = sp // CORES
    core = sp % CORES
    mine = tp // step
    mate = y * CORES + (1 - core)
    side = tp % step
    sign = 2 * side - 1
    other = tp - sign

    def home(j):
        turn = (tp - step * j + 2 * n_tp - 1) % n_tp
        left = turn // near
        place = left * (near - 1 - turn % near) + (1 - left) * (turn % near)
        return step * j + 1 - left, place

    def source(d):
        return (tp + sign * d + n_tp) % n_tp

    def at_y(row):
        return row * CORES + core

    def remote(src, dst, send, recv, **where):
        return pltpu.make_async_remote_copy(
            src_ref=src, dst_ref=dst, send_sem=send, recv_sem=recv, device_id=where, device_id_type=MESH
        )

    def landed(dst, sem):
        pltpu.make_async_copy(dst, dst, sem).wait()

    def columns(n):
        return pl.ds(pl.multiple_of(n * tile, tile), tile)

    loads = [
        pltpu.make_async_copy(pin, ext.at[pl.ds(halo_rows, seg)], lsem.at[0]),
        pltpu.make_async_copy(pool_w, pool_wv, lsem.at[1]),
        pltpu.make_async_copy(out_w, out_wv, lsem.at[2]),
        pltpu.make_async_copy(resid, resbuf, lsem.at[3]),
    ]
    for load in loads:
        load.start()

    with scope("a_barrier"):
        barrier = pltpu.get_barrier_semaphore()
        for d in range(1, n_tp):
            pl.semaphore_signal(barrier, inc=1, device_id={"tp": (tp + d) % n_tp}, device_id_type=MESH)
        for d in range(1, n_y):
            pl.semaphore_signal(barrier, inc=1, device_id={"sp": at_y((y + d) % n_y)}, device_id_type=MESH)
        beside = (sp + 2 * core - 1 + n_sp) % n_sp
        pl.semaphore_signal(barrier, inc=1, device_id={"sp": mate}, device_id_type=MESH)
        pl.semaphore_signal(barrier, inc=1, device_id={"sp": beside}, device_id_type=MESH)
        pl.semaphore_wait(barrier, n_tp + n_y)

    with scope("b_mix"):
        halo = remote(
            pin.at[pl.ds(seg - halo_rows, halo_rows)], ext.at[pl.ds(0, halo_rows)], halo_s, halo_r, sp=(sp + 1) % n_sp
        )
        halo.start()
        loads[0].wait()
        halo.wait()
        at = lax.broadcasted_iota(jnp.int32, (halo_rows + seg, 1), 0)
        own = ext[...].astype(F32)
        own = jnp.where(jnp.logical_and(at < halo_rows, sp == 0), 0.0, own)
        group = tp * channels // GROUP_DIM
        total, picked = own, own
        for level, window in enumerate(pool_windows):
            total = total + pltpu.roll(total, window // 2, 0)
            picked = jnp.where(group == level, total, picked)
        window = lax.shift_left(jnp.int32(2), group.astype(jnp.int32))
        divisor = jnp.minimum(sp * seg + at - halo_rows + 1, window).astype(F32)
        mixed = picked / jnp.maximum(divisor, 1.0) - own
        mixbuf[...] = mixed[halo_rows:].astype(BF16)

    def pool_copy(d):
        to = (tp + d) % n_tp
        return remote(
            mixbuf.at[pl.ds(to * tok, tok)], tokmix.at[tp], pool_sem_s.at[d], pool_sem_r.at[d], tp=to
        )

    keep = pltpu.make_async_copy(mixbuf.at[pl.ds(tp * tok, tok)], tokmix.at[tp], pool_sem_r.at[0])
    keep.start()
    for d in range(1, n_tp):
        pool_copy(d).start()

    with scope("d_route"):
        lanes = whi.shape[1]
        expert_lane = lax.broadcasted_iota(jnp.int32, (tok, 128), 1)
        before = (
            lax.broadcasted_iota(jnp.int32, (tok, tok), 1) < lax.broadcasted_iota(jnp.int32, (tok, tok), 0)
        ).astype(F32).astype(BF16)
        named = [routes[:, k : k + 1] for k in range(TOP)]
        onehot = [(named[k] == expert_lane).astype(F32) for k in range(TOP)]
        earlier = jnp.zeros((1, 128), F32)
        slot_lane = lax.broadcasted_iota(jnp.int32, (1, lanes), 1)
        inside = slot_lane % slots_row
        spill = inside >= row_experts * MAIN
        row_expert = jnp.where(spill, inside - row_experts * MAIN, inside // MAIN)
        slot_rank = jnp.where(spill, MAIN, inside % MAIN).astype(F32)
        valid = jnp.logical_and(row_expert < row_experts, slot_lane < n_y * slots_row)
        slot_expert = jnp.where(valid, slot_lane // slots_row * row_experts + row_expert, -1)
        pick = jnp.zeros((tok, lanes), F32)
        comb = jnp.zeros((tok, lanes), F32)
        for k in range(TOP):
            ranks = dot(before, onehot[k].astype(BF16)) + earlier
            rank = jnp.sum(ranks * onehot[k], axis=1, keepdims=True)
            earlier = earlier + jnp.sum(onehot[k], axis=0, keepdims=True)
            hit = jnp.logical_and(named[k] == slot_expert, rank == slot_rank).astype(F32)
            pick = pick + hit
            comb = comb + hit * route_w[:, k : k + 1]
        high = comb.astype(BF16)
        whi[...] = high
        wlo[...] = (comb - high.astype(F32)).astype(BF16)
        pick_rows = jnp.transpose(pick)[: n_y * slots_row].astype(BF16)

    with scope("e_pool_wait"):
        keep.wait()
        for d in range(1, n_tp):
            pool_copy(d).wait()

    def weight_copies(e):
        col, place = home(core * local_experts + e)
        pairs = [
            (w_gate.at[e], wgu.at[place, :, pl.ds(0, ff)]),
            (w_up.at[e], wgu.at[place, :, pl.ds(ff, ff)]),
            (w_down.at[e], wd.at[pl.ds(place * ff, ff)]),
        ]
        far = lambda: [remote(s, t, w_s.at[e, i], w_r.at[i, place], tp=col) for i, (s, t) in enumerate(pairs)]
        local = lambda: [pltpu.make_async_copy(s, t, w_r.at[i, place]) for i, (s, t) in enumerate(pairs)]
        return col, far, local

    with scope("c_wsend"):
        for e in range(local_experts):
            col, far, local = weight_copies(e)

            @pl.when(col != tp)
            def _():
                for copy in far():
                    copy.start()

            @pl.when(col == tp)
            def _():
                for copy in local():
                    copy.start()

    with scope("e_pool"):
        loads[1].wait()
        per = GROUP_DIM // channels
        for g in range(GROUPS):
            mixed_g = jnp.concatenate([tokmix[g * per + i] for i in range(per)], axis=1)
            cols = slice(g * GROUP_DIM, (g + 1) * GROUP_DIM)
            pooled[:, cols] = (dot(mixed_g, pool_wv[g]) * pool_s[:, cols]).astype(BF16)
        loads[2].wait()

        @pl.loop(0, width // tile)
        def _(n):
            wide[:, columns(n)] = dot(pooled[...], out_wv[:, columns(n)])

    def scaled(values, gain):
        inverse = lax.rsqrt(jnp.mean(values * values, axis=-1, keepdims=True) + norm_eps)
        return values * inverse * gain[...]

    with scope("e_norm"):
        loads[3].wait()

        @pl.loop(0, tok // part)
        def _(r):
            at = pl.ds(pl.multiple_of(r * part, part), part)
            residual = (resbuf[at, :].astype(F32) + scaled(wide[at, :], mix_g)).astype(BF16)
            resbuf[at, :] = residual
            normbuf[at, :] = scaled(residual.astype(F32), ffn_g).astype(BF16)

    with scope("f_disp"):
        @pl.loop(0, width // tile)
        def _(n):
            sent = dot(pick_rows, normbuf[:, columns(n)])
            disp[:, :, :, columns(n)] = sent.reshape(n_y, blocks, 8, tile).astype(BF16)

    by_distance = [d for i in range(1, n_y // 2) for d in (i, n_y - i)] + [n_y // 2]

    def y_copy(d):
        to = (y + d) % n_y
        return remote(disp.at[to], yarr.at[y], y_s.at[d], y_r.at[d], sp=at_y(to))

    y_keep = pltpu.make_async_copy(disp.at[y], yarr.at[y], y_r.at[0])
    y_keep.start()
    for d in by_distance:
        y_copy(d).start()

    order = [mine] + [(mine + i + row_experts) % row_experts for i in (sign, -sign)]
    order = order + [(mine + i) % row_experts for i in range(2, row_experts - 1)]

    def x_copy(k, row, main):
        j = order[k]
        col, place = home(j)
        if main:
            src, at = yarr.at[row, j], row
        else:
            src, at = ovout.at[j], n_y
        dst, sem = rows.at[0, place, at], x_r.at[place, at]
        if k == 0:
            return pltpu.make_async_copy(src, dst, sem)
        return remote(src, dst, x_s.at[k, at], sem, tp=col)

    with scope("f_relay"):
        for d in [0] + by_distance:
            if d == 0:
                y_keep.wait()
            else:
                y_copy(d).wait()
            row = (y - d + n_y) % n_y
            for k in range(row_experts):
                x_copy(k, row, True).start()

    with scope("g_regroup"):
        count = n_y * 8
        to_row = lax.broadcasted_iota(jnp.int32, (row_experts * n_y, count), 0)
        from_row = lax.broadcasted_iota(jnp.int32, (row_experts * n_y, count), 1)
        regroup = (from_row == to_row % n_y * 8 + to_row // n_y).astype(F32).astype(BF16)

        @pl.loop(0, width // tile)
        def _(n):
            moved = dot(regroup, rows_of(yarr[:, row_experts, :, columns(n)]))
            ovout[:, :, columns(n)] = moved.reshape(row_experts, n_y, tile).astype(BF16)

        for k in range(row_experts):
            x_copy(k, n_y, False).start()

    owner = mine // local_experts == core

    def forward_copies(d):
        shard = pl.ds(d * ff, ff)
        return [
            remote(wgu.at[d], wgu.at[d], f_s.at[0, d], f_r.at[0, d], sp=mate),
            remote(wd.at[shard], wd.at[shard], f_s.at[1, d], f_r.at[1, d], sp=mate),
        ]

    with scope("i_weights"):
        @pl.when(owner)
        def _():
            for d in range(near):
                landed(wgu.at[d, :, pl.ds(0, ff)], w_r.at[0, d])
                landed(wgu.at[d, :, pl.ds(ff, ff)], w_r.at[1, d])
                landed(wd.at[pl.ds(d * ff, ff)], w_r.at[2, d])
                for copy in forward_copies(d):
                    copy.start()

    def across(d):
        return remote(rows.at[0, d], rows.at[1, d], n_s.at[d], n_r.at[d], tp=other)

    with scope("i_across"):
        for d in range(near):
            for at in range(held):
                landed(rows.at[0, d, at], x_r.at[d, at])
            across(d).start()

    with scope("i_wmate"):
        @pl.when(jnp.logical_not(owner))
        def _():
            for d in range(near):
                landed(wgu.at[d], f_r.at[0, d])
                landed(wd.at[pl.ds(d * ff, ff)], f_r.at[1, d])

    def partial(d):
        return remote(given.at[d], taken.at[d], p_s.at[d], p_r.at[d], tp=other)

    def out_copy(d):
        return remote(orow.at[d], ret.at[mine], o_s.at[d], o_r.at[mine], tp=source(d))

    pair = 2
    some = 8 * held

    def evaluate(entered, q):
        for i in range(pair):
            d = q * pair + i
            if not entered:
                across(d).wait_recv()
            xb[i * some : (i + 1) * some, :] = rows_of(rows[0 if entered else 1, d])

        @pl.loop(0, near)
        def _(s):
            both = dot(xb[...], wgu[s])
            gate = jnp.minimum(both[:, :ff], clamp_limit)
            linear = jnp.clip(both[:, ff:], -clamp_limit, clamp_limit)
            cols = pl.ds(pl.multiple_of(s * ff, ff), ff)
            act[:, cols] = (gate * jax.nn.sigmoid(glu_alpha * gate) * (linear + 1.0)).astype(BF16)

        @pl.loop(0, width // tile)
        def _(n):
            result = dot(act[...], wd[:, columns(n)])
            for i in range(pair):
                piece = result[i * some : (i + 1) * some]
                if entered:
                    kept[q * pair + i, :, columns(n)] = piece
                else:
                    given[q * pair + i, :, :, columns(n)] = piece.reshape(held, 8, tile).astype(BF16)

        if not entered:
            for i in range(pair):
                partial(q * pair + i).start()

    def finish(q):
        for i in range(pair):
            d = q * pair + i
            partial(d).wait_recv()

            @pl.loop(0, width // tile)
            def _(n):
                both = kept[d, :, columns(n)].reshape(held, 8, tile) + taken[d, :, :, columns(n)].astype(F32)
                orow[d, :, :, columns(n)] = both.astype(BF16)

            if d == 0:
                pltpu.make_async_copy(orow.at[d], ret.at[mine], o_r.at[mine]).start()
            else:
                out_copy(d).start()

    for q in range(near // pair):
        with scope(f"j_near{q}"):
            evaluate(True, q)
        with scope(f"j_far{q}"):
            evaluate(False, q)
        if q:
            with scope(f"j_fin{q - 1}"):
                finish(q - 1)
    with scope("j_fin_last"):
        finish(near // pair - 1)

    def b_copy(k, d):
        to = (y + d) % n_y
        j = order[k]
        src, dst, sem = ret.at[j, to], fin.at[y, j], b_r.at[k, d]
        if d == 0:
            return pltpu.make_async_copy(src, dst, sem)
        return remote(src, dst, b_s.at[k, d], sem, sp=at_y(to))

    def v_copy(d):
        to = (y + d) % n_y
        src, dst, sem = ovback.at[to], fin.at[y, row_experts], v_r.at[d]
        if d == 0:
            return pltpu.make_async_copy(src, dst, sem)
        return remote(src, dst, v_s.at[d], sem, sp=at_y(to))

    with scope("k_back"):
        for k in range(row_experts):
            landed(ret.at[order[k]], o_r.at[order[k]])
            for d in by_distance + [0]:
                b_copy(k, d).start()

    with scope("l_back"):
        to_row = lax.broadcasted_iota(jnp.int32, (count, row_experts * n_y), 0)
        from_row = lax.broadcasted_iota(jnp.int32, (count, row_experts * n_y), 1)
        regroup_back = (from_row == to_row % 8 * n_y + to_row // 8).astype(F32)
        regroup_back = jnp.where(to_row % 8 < row_experts, regroup_back, 0.0).astype(BF16)

        @pl.loop(0, width // tile)
        def _(n):
            moved = dot(regroup_back, rows_of(ret[:, n_y, :, columns(n)]))
            ovback[:, :, columns(n)] = moved.reshape(n_y, 8, tile).astype(BF16)

        for d in by_distance + [0]:
            v_copy(d).start()

    with scope("m_finwait"):
        for d in [0] + by_distance:
            for k in range(row_experts):
                b_copy(k, d).wait()
            v_copy(d).wait()

    with scope("n_comb"):
        @pl.loop(0, width // tile)
        def _(n):
            came = rows_of(fin[:, :, :, columns(n)])
            came = jnp.concatenate([came, jnp.zeros((lanes - n_y * slots_row, tile), BF16)], axis=0)
            wide[:, columns(n)] = dot(whi[...], came) + dot(wlo[...], came)

        @pl.loop(0, tok // part)
        def _(r):
            at = pl.ds(pl.multiple_of(r * part, part), part)
            outbuf[at, :] = (resbuf[at, :].astype(F32) + scaled(wide[at, :], post_g)).astype(BF16)

        result = pltpu.make_async_copy(outbuf, out, lsem.at[0])
        result.start()

    with scope("o_drain"):
        for e in range(local_experts):
            col, far, local = weight_copies(e)

            @pl.when(col != tp)
            def _():
                for copy in far():
                    copy.wait_send()

        for k in range(1, row_experts):
            for row in range(n_y):
                x_copy(k, row, True).wait_send()
            x_copy(k, n_y, False).wait_send()

        @pl.when(owner)
        def _():
            for d in range(near):
                for copy in forward_copies(d):
                    copy.wait_send()

        for d in range(near):
            across(d).wait_send()
            partial(d).wait_send()
            if d:
                out_copy(d).wait_send()
        result.wait()


def per_device(
    resid_in, pool_input, pool_weight, pool_scale, out_weight, mix_gain, ffn_gain,
    w_gate, w_up, w_down, routes, route_weight, post_gain,
):
    n_sp = lax.axis_size("sp")
    n_tp = lax.axis_size("tp")
    n_y = n_sp // CORES
    seg, channels = pool_input.shape
    tok, width = resid_in.shape
    local_experts, _, ff = w_gate.shape
    row_experts = local_experts * CORES
    blocks = row_experts + 1
    slots = n_y * blocks * 8
    lanes = -(-slots // 128) * 128
    held = n_y + 1
    near = row_experts
    dma = pltpu.SemaphoreType.DMA
    vmem = pltpu.VMEM
    whole = pl.BlockSpec(memory_space=pltpu.VMEM)
    there = pl.BlockSpec(memory_space=pl.ANY)
    scratch = [
        vmem((halo_rows + seg, channels), BF16),
        vmem((seg, channels), BF16),
        vmem((n_tp, tok, channels), BF16),
        vmem(pool_weight.shape, BF16),
        vmem(out_weight.shape, BF16),
        vmem((tok, pool_scale.shape[0]), BF16),
        vmem((tok, width), F32),
        vmem((tok, width), BF16),
        vmem((tok, width), BF16),
        vmem((tok, lanes), BF16),
        vmem((tok, lanes), BF16),
        vmem((n_y, blocks, 8, width), BF16),
        vmem((n_y, blocks, 8, width), BF16),
        vmem((row_experts, 8, width), BF16),
        vmem((near, width, 2 * ff), BF16),
        vmem((near * ff, width), BF16),
        vmem((2, near, held, 8, width), BF16),
        vmem((2 * held * 8, width), BF16),
        vmem((2 * held * 8, near * ff), BF16),
        vmem((near, held * 8, width), F32),
        vmem((near, held, 8, width), BF16),
        vmem((near, held, 8, width), BF16),
        vmem((near, held, 8, width), BF16),
        vmem((row_experts, held, 8, width), BF16),
        vmem((n_y, 8, width), BF16),
        vmem((n_y, blocks, 8, width), BF16),
        vmem((tok, width), BF16),
        dma((4,)), dma, dma, dma((n_tp,)), dma((n_tp,)),
        dma((local_experts, 3)), dma((3, near)), dma((2, near)), dma((2, near)),
        dma((n_y,)), dma((n_y,)), dma((row_experts, held)), dma((near, held)),
        dma((near,)), dma((near,)), dma((near,)), dma((near,)),
        dma((near,)), dma((row_experts,)), dma((row_experts, n_y)), dma((row_experts, n_y)), dma((n_y,)), dma((n_y,)),
    ]
    return pl.pallas_call(
        functools.partial(kernel, n_sp, n_tp),
        out_shape=jax.ShapeDtypeStruct((tok, width), BF16),
        in_specs=[there, there, there, whole, there, whole, whole, there, there, there, whole, whole, whole],
        out_specs=there,
        scratch_shapes=scratch,
        compiler_params=pltpu.CompilerParams(
            collective_id=0, has_side_effects=True, vmem_limit_bytes=60 * 1024 * 1024
        ),
    )(
        pool_input, resid_in, pool_weight, pool_scale[None], out_weight, mix_gain[None], ffn_gain[None],
        w_gate, w_up, w_down, routes, route_weight, post_gain[None],
    )


def solution(mesh):
    in_specs = (
        P(("grp", "sp", "tp"), None),
        P(("grp", "sp"), "tp"),
        P(),
        P(),
        P(),
        P(),
        P(),
        P("sp", None, "tp"),
        P("sp", None, "tp"),
        P("sp", "tp", None),
        P(("grp", "sp", "tp"), None),
        P(("grp", "sp", "tp"), None),
        P(),
    )
    out_specs = P(("grp", "sp", "tp"), None)
    return jax.shard_map(
        per_device, mesh=mesh, in_specs=in_specs, out_specs=out_specs, check_vma=False
    )
```

time: 398 us -> 219 us (0.55)
  waiting for transfers between devices: 234 us -> 0 us
  Pallas kernels: 0 us -> 214 us
  blocking collectives: 91.7 us -> 0 us
  matrix products: 20.2 us -> 0 us
  local copies, waits for them, and re-layouts: 23 us -> 4.7 us
  between operations: 13.7 us -> 0.01 us
  starting transfers between devices: 9.79 us -> 0 us
  other arithmetic: 4.91 us -> 0 us
    pallas_call x0 -> x1, Pallas kernels: none -> 214 us  [per_device(): pl.pallas_call(functools.partial(kernel, n_sp, n_tp), out_shape=jax.Shape...]
    reduce_scatter x1 -> x0, waiting for transfers between devices: 105 us -> none  [per_device(): lax.psum_scatter(terms.reshape(1 * lax.axis_size('tp'), n_sp, local_exper...]
    all_gather x1 -> x0, waiting for transfers between devices: 104 us -> none  [per_device(): arrived = lax.all_gather(at_owner[:, None], 'tp', axis=1, tiled=True)]
    all_to_all x2 -> x0, blocking collectives: 91.7 us -> none  [the longest x1 47.2 us: per_device(): lax.all_to_all(results, 'sp', split_axis=0, concat_axis=0, tiled=True)]
    dot_general x7 -> x0, matrix products: 20.2 us -> none  [the longest x1 5.33 us: per_device(): jnp.einsum('sklcd,ldf->sklcf', arrived, w_gate, preferred_element_type=jn...]
    ppermute x1 -> x0, waiting for transfers between devices: 15 us -> none  [passed_along(): return lax.ppermute(x, axis, pairs)]
    convert_element_type x3 -> x0, local copies, waits for them, and re-layouts: 14.7 us -> none  [the longest x1 12.5 us: per_device(): terms.reshape(1 * lax.axis_size('tp'), n_sp, local_experts * CAP, width)]
    all_to_all x1 -> x0, waiting for transfers between devices: 9.42 us -> none  [per_device(): lax.all_to_all(mixed_rows, 'tp', split_axis=0, concat_axis=1, tiled=True)]
  transfers between devices with their start and end apart: 4 -> 0, of which waited for: 4 -> 0; matrix products, arithmetic and copies ran while one was open for 1% -> 0% of each run, Pallas kernels for 0% -> 0%
where the time goes in v2:
time: 219 us
  Pallas kernels  214 us (98%)
  local copies, waits for them, and re-layouts  4.7 us (2%)
    pallas_call x1, Pallas kernels, per_device(): pl.pallas_call(functools.partial(kernel, n_sp, n_tp), out_shape=jax.Shape...  214 us
    unnamed x3, local copies, waits for them, and re-layouts  4.7 us

profile of v2, /device:TPU:513, one launch (start us, length us, event | category | flops | bytes accessed | tf_op | source)
XLA Modules:
  0.0 219.0 jit_solution(11668750335247473438)
XLA Ops:
  0.0 1.4 copy.14.routes
  1.4 1.4 copy.15.route_w
  2.8 214.3 %shard_map.127 = bf16[128,2048]{1,0:T(8,128)(2,1)} custom-call(bf16[1024,128]{1,0:T(8,128)(2,1)} %pin.1, bf16[128,2048]{1,0:T(8,128)(2,1)} %resid.1, bf16[4,256,256]{2,1,0:T(8,128)(2,1)} %pool_w.1, f32[1,1024]{1,0:T(1,128)} %bitcast.7, bf16[1024,2048]{1,0:T(8,128)(2,1)} %out_w.1, f32[1,2048]{1,0:T(1,128)} %bitcast.4, f32[1,2048]{1,0:T(1,128)} %bitcast.5, ...), custom_call_target="tpu_custom_call" | custom-call | tf_op jit(solution)/shard_map/pallas_call | solution.py:523
  217.1 1.9 copy.17

commit v3 on v2

--- a/solution.py
+++ b/solution.py
@@ -38,9 +38,9 @@
     pin, resid, pool_w, pool_s, out_w, mix_g, ffn_g, w_gate, w_up, w_down, routes, route_w, post_g,
     out,
     ext, mixbuf, tokmix, pool_wv, out_wv, pooled, wide, resbuf, normbuf, whi, wlo,
-    disp, yarr, ovout, wgu, wd, rows, xb, act, kept, given, taken, orow, ret, ovback, fin, outbuf,
+    disp, yarr, ovout, wgu, wd, rows, xb, act, orow, ret, ovback, fin, outbuf,
     lsem, halo_s, halo_r, pool_sem_s, pool_sem_r, w_s, w_r, f_s, f_r,
-    y_s, y_r, x_s, x_r, n_s, n_r, p_s, p_r, o_s, o_r, b_s, b_r, v_s, v_r,
+    z_s, z_r, q_s, q_r, y_s, y_r, x_s, x_r, o_s, o_r, b_s, b_r, v_s, v_r,
 ):
     n_y = n_sp // CORES
     local_experts = w_gate.shape[0]
@@ -62,6 +62,9 @@
     core = sp % CORES
     mine = tp // step
     mate = y * CORES + (1 - core)
+    grp = lax.axis_index("grp")
+    half = grp % 2
+    twin = grp + 1 - 2 * half
     side = tp % step
     sign = 2 * side - 1
     other = tp - sign
@@ -107,7 +110,8 @@
         beside = (sp + 2 * core - 1 + n_sp) % n_sp
         pl.semaphore_signal(barrier, inc=1, device_id={"sp": mate}, device_id_type=MESH)
         pl.semaphore_signal(barrier, inc=1, device_id={"sp": beside}, device_id_type=MESH)
-        pl.semaphore_wait(barrier, n_tp + n_y)
+        pl.semaphore_signal(barrier, inc=1, device_id={"grp": twin}, device_id_type=MESH)
+        pl.semaphore_wait(barrier, n_tp + n_y + 1)
 
     with scope("b_mix"):
         halo = remote(
@@ -175,30 +179,121 @@
         for d in range(1, n_tp):
             pool_copy(d).wait()
 
-    def weight_copies(e):
+    owner = mine // local_experts == core
+    items = 3
+    deep = width // 4
+    short = ff // 2
+
+    def item(slot, which, i):
+        if i == items - 1:
+            return wd.at[pl.ds(slot * ff + which * short, short)]
+        return wgu.at[slot, pl.ds(which * 2 * deep + i * deep, deep)]
+
+    def both_whole(slot):
+        return wgu.at[slot], wd.at[pl.ds(slot * ff, ff)]
+
+    def weight_copies(e, i):
         col, place = home(core * local_experts + e)
+        slot = col % step * near + place
+        if i == items - 1:
+            pairs = [(w_down.at[e, pl.ds(half * short, short)], item(slot, half, i))]
+        else:
+            at = pl.ds(half * 2 * deep + i * deep, deep)
+            pairs = [
+                (w_gate.at[e, at], wgu.at[slot, at, pl.ds(0, ff)]),
+                (w_up.at[e, at], wgu.at[slot, at, pl.ds(ff, ff)]),
+            ]
+        far = lambda: [remote(s, t, w_s.at[e, i, n], w_r.at[i, place], tp=col) for n, (s, t) in enumerate(pairs)]
+        return col, far
+
+    def own_shard():
+        slot = side * near
+        e = mine % local_experts
         pairs = [
-            (w_gate.at[e], wgu.at[place, :, pl.ds(0, ff)]),
-            (w_up.at[e], wgu.at[place, :, pl.ds(ff, ff)]),
-            (w_down.at[e], wd.at[pl.ds(place * ff, ff)]),
+            (w_gate.at[e], wgu.at[slot, :, pl.ds(0, ff)]),
+            (w_up.at[e], wgu.at[slot, :, pl.ds(ff, ff)]),
+            (w_down.at[e], wd.at[pl.ds(slot * ff, ff)]),
         ]
-        far = lambda: [remote(s, t, w_s.at[e, i], w_r.at[i, place], tp=col) for i, (s, t) in enumerate(pairs)]
-        local = lambda: [pltpu.make_async_copy(s, t, w_r.at[i, place]) for i, (s, t) in enumerate(pairs)]
-        return col, far, local
+        local = lambda: [pltpu.make_async_copy(s, t, w_r.at[n, 0]) for n, (s, t) in enumerate(pairs)]
+        over = lambda: [remote(s, t, q_s.at[n, 0], q_r.at[n, 0], tp=other) for n, (s, t) in enumerate(pairs)]
+        return local, over
 
     with scope("c_wsend"):
-        for e in range(local_experts):
-            col, far, local = weight_copies(e)
-
-            @pl.when(col != tp)
-            def _():
-                for copy in far():
-                    copy.start()
-
-            @pl.when(col == tp)
-            def _():
-                for copy in local():
-                    copy.start()
+        @pl.when(owner)
+        def _():
+            local, over = own_shard()
+            for copy in local() + over():
+                copy.start()
+
+        for i in range(items):
+            for e in range(local_experts):
+                col, far = weight_copies(e, i)
+
+                @pl.when(col != tp)
+                def _():
+                    for copy in far():
+                        copy.start()
+
+    def swap_copy(at_side, d, i):
+        src = item(at_side * near + d, half, i)
+        rel = (at_side - side) * (at_side - side)
+        return remote(src, src, z_s.at[rel, d, i], z_r.at[rel, d, i], grp=twin)
+
+    def over_copy(d, i):
+        src = item(side * near + d, half, i)
+        return remote(src, src, q_s.at[i, d], q_r.at[i, d], tp=other)
+
+    def mate_copy(at_side, d, which, i):
+        slot = at_side * near + d
+        rel = (at_side - side) * (at_side - side)
+        src = item(slot, half if which == 0 else 1 - half, i) if d else both_whole(slot)[i]
+        return remote(src, src, f_s.at[rel, d, which, i], f_r.at[rel, d, which, i], sp=mate)
+
+    def own_came():
+        @pl.when(owner)
+        def _():
+            slot = side * near
+            landed(wgu.at[slot, :, pl.ds(0, ff)], w_r.at[0, 0])
+            landed(wgu.at[slot, :, pl.ds(ff, ff)], w_r.at[1, 0])
+            landed(wd.at[pl.ds(slot * ff, ff)], w_r.at[2, 0])
+            for i in range(2):
+                mate_copy(side, 0, 0, i).start()
+
+    def over_own_came():
+        @pl.when(owner)
+        def _():
+            slot = (1 - side) * near
+            landed(wgu.at[slot, :, pl.ds(0, ff)], q_r.at[0, 0])
+            landed(wgu.at[slot, :, pl.ds(ff, ff)], q_r.at[1, 0])
+            landed(wd.at[pl.ds(slot * ff, ff)], q_r.at[2, 0])
+            for i in range(2):
+                mate_copy(1 - side, 0, 0, i).start()
+
+    def came(i):
+        @pl.when(owner)
+        def _():
+            for d in range(1, near):
+                landed(item(side * near + d, half, i), w_r.at[i, d])
+                over_copy(d, i).start()
+                swap_copy(side, d, i).start()
+                mate_copy(side, d, 0, i).start()
+
+    def over_came(i):
+        @pl.when(owner)
+        def _():
+            for d in range(1, near):
+                landed(item((1 - side) * near + d, half, i), q_r.at[i, d])
+                swap_copy(1 - side, d, i).start()
+                mate_copy(1 - side, d, 0, i).start()
+
+    def swap_came(i):
+        @pl.when(owner)
+        def _():
+            for rel in range(2):
+                at_side = side + rel - 2 * rel * side
+                for d in range(1, near):
+                    landed(item(at_side * near + d, 1 - half, i), z_r.at[rel, d, i])
+                    mate_copy(at_side, d, 1, i).start()
 
     with scope("e_pool"):
         loads[1].wait()
@@ -254,7 +349,7 @@
             src, at = yarr.at[row, j], row
         else:
             src, at = ovout.at[j], n_y
-        dst, sem = rows.at[0, place, at], x_r.at[place, at]
+        dst, sem = rows.at[place, at], x_r.at[place, at]
         if k == 0:
             return pltpu.make_async_copy(src, dst, sem)
         return remote(src, dst, x_s.at[k, at], sem, tp=col)
@@ -268,6 +363,17 @@
             row = (y - d + n_y) % n_y
             for k in range(row_experts):
                 x_copy(k, row, True).start()
+            if d == 0:
+                own_came()
+            elif d == by_distance[1]:
+                came(0)
+            elif d == by_distance[3]:
+                over_own_came()
+                came(1)
+                over_came(0)
+            elif d == by_distance[5]:
+                came(2)
+                over_came(1)
 
     with scope("g_regroup"):
         count = n_y * 8
@@ -283,43 +389,23 @@
         for k in range(row_experts):
             x_copy(k, n_y, False).start()
 
-    owner = mine // local_experts == core
-
-    def forward_copies(d):
-        shard = pl.ds(d * ff, ff)
-        return [
-            remote(wgu.at[d], wgu.at[d], f_s.at[0, d], f_r.at[0, d], sp=mate),
-            remote(wd.at[shard], wd.at[shard], f_s.at[1, d], f_r.at[1, d], sp=mate),
-        ]
-
     with scope("i_weights"):
-        @pl.when(owner)
-        def _():
-            for d in range(near):
-                landed(wgu.at[d, :, pl.ds(0, ff)], w_r.at[0, d])
-                landed(wgu.at[d, :, pl.ds(ff, ff)], w_r.at[1, d])
-                landed(wd.at[pl.ds(d * ff, ff)], w_r.at[2, d])
-                for copy in forward_copies(d):
-                    copy.start()
-
-    def across(d):
-        return remote(rows.at[0, d], rows.at[1, d], n_s.at[d], n_r.at[d], tp=other)
-
-    with scope("i_across"):
-        for d in range(near):
-            for at in range(held):
-                landed(rows.at[0, d, at], x_r.at[d, at])
-            across(d).start()
+        over_came(2)
+        for i in range(items):
+            swap_came(i)
 
     with scope("i_wmate"):
         @pl.when(jnp.logical_not(owner))
         def _():
-            for d in range(near):
-                landed(wgu.at[d], f_r.at[0, d])
-                landed(wd.at[pl.ds(d * ff, ff)], f_r.at[1, d])
-
-    def partial(d):
-        return remote(given.at[d], taken.at[d], p_s.at[d], p_r.at[d], tp=other)
+            for rel in range(2):
+                at_side = side + rel - 2 * rel * side
+                for i, piece in enumerate(both_whole(at_side * near)):
+                    landed(piece, f_r.at[rel, 0, 0, i])
+                for which in range(2):
+                    for d in range(1, near):
+                        for i in range(items):
+                            piece = item(at_side * near + d, half if which == 0 else 1 - half, i)
+                            landed(piece, f_r.at[rel, d, which, i])
 
     def out_copy(d):
         return remote(orow.at[d], ret.at[mine], o_s.at[d], o_r.at[mine], tp=source(d))
@@ -327,14 +413,14 @@
     pair = 2
     some = 8 * held
 
-    def evaluate(entered, q):
+    def evaluate(q):
         for i in range(pair):
             d = q * pair + i
-            if not entered:
-                across(d).wait_recv()
-            xb[i * some : (i + 1) * some, :] = rows_of(rows[0 if entered else 1, d])
-
-        @pl.loop(0, near)
+            for at in range(held):
+                landed(rows.at[d, at], x_r.at[d, at])
+            xb[i * some : (i + 1) * some, :] = rows_of(rows[d])
+
+        @pl.loop(0, n_tp)
         def _(s):
             both = dot(xb[...], wgu[s])
             gate = jnp.minimum(both[:, :ff], clamp_limit)
@@ -347,40 +433,23 @@
             result = dot(act[...], wd[:, columns(n)])
             for i in range(pair):
                 piece = result[i * some : (i + 1) * some]
-                if entered:
-                    kept[q * pair + i, :, columns(n)] = piece
-                else:
-                    given[q * pair + i, :, :, columns(n)] = piece.reshape(held, 8, tile).astype(BF16)
-
-        if not entered:
-            for i in range(pair):
-                partial(q * pair + i).start()
-
-    def finish(q):
+                orow[q * pair + i, :, :, columns(n)] = piece.reshape(held, 8, tile).astype(BF16)
+
         for i in range(pair):
             d = q * pair + i
-            partial(d).wait_recv()
-
-            @pl.loop(0, width // tile)
-            def _(n):
-                both = kept[d, :, columns(n)].reshape(held, 8, tile) + taken[d, :, :, columns(n)].astype(F32)
-                orow[d, :, :, columns(n)] = both.astype(BF16)
-
             if d == 0:
                 pltpu.make_async_copy(orow.at[d], ret.at[mine], o_r.at[mine]).start()
             else:
                 out_copy(d).start()
 
     for q in range(near // pair):
-        with scope(f"j_near{q}"):
-            evaluate(True, q)
-        with scope(f"j_far{q}"):
-            evaluate(False, q)
-        if q:
-            with scope(f"j_fin{q - 1}"):
-                finish(q - 1)
-    with scope("j_fin_last"):
-        finish(near // pair - 1)
+        with scope(f"j_eval{q}"):
+            evaluate(q)
+
+    def back(k):
+        landed(ret.at[order[k]], o_r.at[order[k]])
+        for d in by_distance + [0]:
+            b_copy(k, d).start()
 
     def b_copy(k, d):
         to = (y + d) % n_y
@@ -397,11 +466,10 @@
             return pltpu.make_async_copy(src, dst, sem)
         return remote(src, dst, v_s.at[d], sem, sp=at_y(to))
 
-    with scope("k_back"):
-        for k in range(row_experts):
-            landed(ret.at[order[k]], o_r.at[order[k]])
-            for d in by_distance + [0]:
-                b_copy(k, d).start()
+    for q in range(near // pair):
+        with scope(f"k_back{q}"):
+            for k in range(q * pair, (q + 1) * pair):
+                back(k)
 
     with scope("l_back"):
         to_row = lax.broadcasted_iota(jnp.int32, (count, row_experts * n_y), 0)
@@ -439,13 +507,14 @@
         result.start()
 
     with scope("o_drain"):
-        for e in range(local_experts):
-            col, far, local = weight_copies(e)
-
-            @pl.when(col != tp)
-            def _():
-                for copy in far():
-                    copy.wait_send()
+        for i in range(items):
+            for e in range(local_experts):
+                col, far = weight_copies(e, i)
+
+                @pl.when(col != tp)
+                def _():
+                    for copy in far():
+                        copy.wait_send()
 
         for k in range(1, row_experts):
             for row in range(n_y):
@@ -454,15 +523,22 @@
 
         @pl.when(owner)
         def _():
-            for d in range(near):
-                for copy in forward_copies(d):
-                    copy.wait_send()
-
-        for d in range(near):
-            across(d).wait_send()
-            partial(d).wait_send()
-            if d:
-                out_copy(d).wait_send()
+            for copy in own_shard()[1]():
+                copy.wait_send()
+            for rel in range(2):
+                at_side = side + rel - 2 * rel * side
+                for i in range(2):
+                    mate_copy(at_side, 0, 0, i).wait_send()
+                for d in range(1, near):
+                    for i in range(items):
+                        if rel == 0:
+                            over_copy(d, i).wait_send()
+                        swap_copy(at_side, d, i).wait_send()
+                        for which in range(2):
+                            mate_copy(at_side, d, which, i).wait_send()
+
+        for d in range(1, near):
+            out_copy(d).wait_send()
         result.wait()
 
 
@@ -501,23 +577,20 @@
         vmem((n_y, blocks, 8, width), BF16),
         vmem((n_y, blocks, 8, width), BF16),
         vmem((row_experts, 8, width), BF16),
-        vmem((near, width, 2 * ff), BF16),
-        vmem((near * ff, width), BF16),
-        vmem((2, near, held, 8, width), BF16),
+        vmem((n_tp, width, 2 * ff), BF16),
+        vmem((n_tp * ff, width), BF16),
+        vmem((near, held, 8, width), BF16),
         vmem((2 * held * 8, width), BF16),
-        vmem((2 * held * 8, near * ff), BF16),
-        vmem((near, held * 8, width), F32),
-        vmem((near, held, 8, width), BF16),
-        vmem((near, held, 8, width), BF16),
+        vmem((2 * held * 8, n_tp * ff), BF16),
         vmem((near, held, 8, width), BF16),
         vmem((row_experts, held, 8, width), BF16),
         vmem((n_y, 8, width), BF16),
         vmem((n_y, blocks, 8, width), BF16),
         vmem((tok, width), BF16),
         dma((4,)), dma, dma, dma((n_tp,)), dma((n_tp,)),
-        dma((local_experts, 3)), dma((3, near)), dma((2, near)), dma((2, near)),
+        dma((local_experts, 3, 2)), dma((3, near)), dma((2, near, 2, 3)), dma((2, near, 2, 3)),
+        dma((2, near, 3)), dma((2, near, 3)), dma((3, near)), dma((3, near)),
         dma((n_y,)), dma((n_y,)), dma((row_experts, held)), dma((near, held)),
-        dma((near,)), dma((near,)), dma((near,)), dma((near,)),
         dma((near,)), dma((row_experts,)), dma((row_experts, n_y)), dma((row_experts, n_y)), dma((n_y,)), dma((n_y,)),
     ]
     return pl.pallas_call(

time: 219 us -> 180 us (0.82)
  the two profiles are of different devices: /device:TPU:513 before, /device:TPU:521 now
where the time goes in v3:
time: 180 us; the launch traced here: 179 us
  Pallas kernels  175 us (97%)
  local copies, waits for them, and re-layouts  4.7 us (3%)
    pallas_call x1, Pallas kernels, per_device(): pl.pallas_call(functools.partial(kernel, n_sp, n_tp), out_shape=jax.Shape...  175 us
    unnamed x3, local copies, waits for them, and re-layouts  4.7 us

profile of v3, /device:TPU:521, one launch (start us, length us, event | category | flops | bytes accessed | tf_op | source)
XLA Modules:
  0.0 179.4 jit_solution(17593706062404734307)
XLA Ops:
  0.0 1.4 copy.14.routes
  1.4 1.4 copy.15.route_w
  2.8 174.7 %shard_map.127 = bf16[128,2048]{1,0:T(8,128)(2,1)} custom-call(bf16[1024,128]{1,0:T(8,128)(2,1)} %pin.1, bf16[128,2048]{1,0:T(8,128)(2,1)} %resid.1, bf16[4,256,256]{2,1,0:T(8,128)(2,1)} %pool_w.1, f32[1,1024]{1,0:T(1,128)} %bitcast.7, bf16[1024,2048]{1,0:T(8,128)(2,1)} %out_w.1, f32[1,2048]{1,0:T(1,128)} %bitcast.4, f32[1,2048]{1,0:T(1,128)} %bitcast.5, ...), custom_call_target="tpu_custom_call" | custom-call | tf_op jit(solution)/shard_map/pallas_call | solution.py:596
  177.5 1.9 %copy.17 = bf16[128,2048]{1,0:T(8,128)(2,1)} copy(bf16[128,2048]{1,0:T(8,128)(2,1)} %shard_map.127) | data formatting | bytes 1048576
